TPU v7x, 32 devices: a whole 2x2x4 slice. The times are simulated.
32 devices in a mesh: ep: 4 (over z), tp: 8 (over y, x, core).
Axes of the slice: x: 2, y: 2, z: 4, core: 2. Of those that a mesh axis runs over, the one named last changes fastest.
Arguments:
- tokens: bfloat16 [512, 2048], P('ep'), may hold values from -6 to 6
- norm_gain: float32 [2048], replicated, may hold values from 0.1 to 1.9
- route_ids: int32 [512, 2], P('ep'), may hold values from 0 to 3, all different within a row; in each aligned block of 128 rows (0 to 127, 128 to 255, ...) at most 96 rows name the same one
- route_weights: float32 [512, 2], P('ep'), may hold values from 0.05 to 1
- gate_proj: bfloat16 [4, 2048, 12288], P('ep', None, 'tp'), may hold values from -0.125 to 0.125
- up_proj: bfloat16 [4, 2048, 12288], P('ep', None, 'tp'), may hold values from -0.125 to 0.125
- down_proj: bfloat16 [4, 12288, 2048], P('ep', 'tp'), may hold values from -0.0546875 to 0.0546875
Outputs:
- mixed: bfloat16 [512, 2048], P('ep', 'tp')
Inputs may be any that keep to these rules, and one draw needn't show every extreme that they name: `route_ids`: each token names 2 different experts; within the rows of one device (aligned blocks of 128 tokens) no expert is named by more than 96 pairs, a bound that some block reaches.
All inputs are finite; a program needn't handle non-finite values.
Results may differ from a plain program's by a relative error of at most 0.017.
Values may be sent and summed in bfloat16 or wider, within the bound.
A program may use at most 64 MiB of HBM per device.

v0:
```python
import jax
import jax.numpy as jnp
from jax import lax
from jax.sharding import PartitionSpec as P


def local(tokens, norm_gain, route_ids, route_weights, gate_proj, up_proj, down_proj):
    ep_count = lax.axis_size("ep")
    tp_count = lax.axis_size("tp")
    tok_rows, width = tokens.shape
    topk = route_ids.shape[1]
    capacity = min(tok_rows, (3 * tok_rows * topk + 2 * ep_count - 1) // (2 * ep_count))
    share_width = width // tp_count
    values = tokens.astype(jnp.float32)
    mean_square = jnp.mean(values * values, axis=-1, keepdims=True)
    normed = (values * lax.rsqrt(mean_square + 1e-06) * norm_gain).astype(jnp.bfloat16)
    route_flat = route_ids.reshape(-1)
    onehot = (route_flat[:, None] == jnp.arange(ep_count, dtype=jnp.int32)[None, :]).astype(
        jnp.int32
    )
    slot_index = jnp.sum((jnp.cumsum(onehot, axis=0) - onehot) * onehot, axis=1)
    repeated = jnp.repeat(normed, topk, axis=0)
    down_local = down_proj[0]
    outgoing = (
        jnp.zeros((ep_count, capacity, width), jnp.bfloat16)
        .at[route_flat, slot_index]
        .set(repeated)
    )
    arrived = lax.all_to_all(outgoing, "ep", split_axis=0, concat_axis=0, tiled=True)
    item_rows = arrived.shape[1]
    merged_rows = arrived.reshape(-1, width)
    gate_act = jnp.dot(merged_rows, gate_proj[0], preferred_element_type=jnp.float32)
    up_act = jnp.dot(merged_rows, up_proj[0], preferred_element_type=jnp.float32)
    hidden = (jax.nn.silu(gate_act) * up_act).astype(jnp.bfloat16)
    term = lax.dot_general(
        down_local, hidden, (((0,), (1,)), ((), ())), preferred_element_type=jnp.float32
    )
    term = lax.optimization_barrier(term.astype(jnp.bfloat16))
    summed = lax.psum_scatter(
        term.astype(jnp.float32).astype(jnp.bfloat16), "tp", scatter_dimension=0, tiled=True
    ).astype(jnp.float32)
    back = summed.T.reshape(ep_count, item_rows, share_width)
    returned = lax.all_to_all(
        back.astype(jnp.bfloat16), "ep", split_axis=0, concat_axis=0, tiled=True
    ).astype(back.dtype)
    columns_back = returned.shape[2]
    picked = returned[route_flat, slot_index].reshape(tok_rows, topk, columns_back)
    weighted = jnp.sum(route_weights[:, :, None] * picked, axis=1)
    return weighted.astype(jnp.bfloat16)


def solution(mesh):
    placed = (
        P("ep", None),
        P(),
        P("ep", None),
        P("ep", None),
        P("ep", None, "tp"),
        P("ep", None, "tp"),
        P("ep", "tp", None),
    )
    return jax.shard_map(
        local, mesh=mesh, in_specs=placed, out_specs=P("ep", "tp"), check_vma=False
    )
```

profile of v0, /device:TPU:0, one launch (start us, length us, event | category | flops | bytes accessed | tf_op | source)
XLA Modules:
  0.0 157.4 jit_solution(11334594695858422979)
XLA Ops:
  6.5 0.8 copy.12
  7.3 0.1 eq.29
  7.5 0.1 eq.25
  7.6 0.1 reshape.82
  7.8 1.2 reduce-window.6
  9.0 0.1 slice.12
  9.1 0.1 copy.15
  9.2 0.1 copy.16
  9.4 1.2 fusion.18
  10.6 1.2 fusion.20
  11.9 0.6 broadcast_in_dim.5
  12.5 0.4 reshape.95
  13.0 0.2 broadcast_in_dim.4
  13.2 23.1 %scatter_fusion = bf16[4,96,2048]{2,1,0:T(8,128)(2,1)S(1)} fusion(bf16[4,96,2048]{2,1,0:T(8,128)(2,1)S(1)} %broadcast_in_dim.4, s32[256]{0:T(256)S(1)} %bitcast.49, bf16[256,2048]{1,0:T(8,128)(2,1)S(1)} %reshape.95), kind=kCustom, calls=%fused_computation.1 | custom fusion | bytes 3147776 | tf_op jit(solution)/shard_map/scatter | solution.py:27
  36.3 43.1 %all_to_all.10 = bf16[4,96,2048]{2,1,0:T(8,128)(2,1)S(1)} all-to-all(bf16[4,96,2048]{2,1,0:T(8,128)(2,1)S(1)} %scatter_fusion), channel_id=1, replica_groups=mesh['ep'=4,'tp'=8] {'ep'}, dimensions={0} | all-to-all | bytes 3145728 | tf_op jit(solution)/shard_map/all_to_all | solution.py:29
  79.4 6.8 %fusion.4 = f32[384,1536]{1,0:T(8,128)} fusion(bf16[384,2048]{1,0:T(8,128)(2,1)S(1)} %bitcast.51, bf16[1,2048,1536]{2,1,0:T(8,128)(2,1)} %param.11), kind=kOutput, calls=%fused_computation.6 | convolution fusion | flops 2415919104 | bytes 10223616 | tf_op jit(solution)/shard_map/dot_general | solution.py:32
  86.2 11.6 %fusion.15 = bf16[2048,384]{0,1:T(8,128)(2,1)} fusion(bf16[1,1536,2048]{2,1,0:T(8,128)(2,1)} %param.13, bf16[384,2048]{1,0:T(8,128)(2,1)S(1)} %bitcast.52, bf16[1,2048,1536]{2,1,0:T(8,128)(2,1)} %param.12, f32[384,1536]{1,0:T(8,128)} %fusion.4), kind=kOutput, calls=%fused_computation.11 | convolution fusion | flops 4836163584 | bytes 18087936 | tf_op jit(solution)/shard_map/dot_general | solution.py:35
  97.8 37.6 %reduce-scatter.2.cloned.1.call-done = bf16[256,384]{0,1:T(8,128)(2,1)} async-done(((bf16[2048,384]{0,1:T(8,128)(2,1)}), bf16[256,384]{0,1:T(8,128)(2,1)}) %reduce-scatter.2.cloned.1.call-update) | async-done | bytes 196624 | tf_op jit(solution)/shard_map/reduce_scatter | solution.py:39
  135.4 4.6 %all-to-all-start.1 = ((bf16[4,96,256]{2,1,0:T(8,128)(2,1)}), bf16[4,96,256]{2,1,0:T(8,128)(2,1)S(1)}, u32[]{:S(2)}, u32[]{:S(2)}) async-start(bf16[4,96,256]{2,1,0:T(8,128)(2,1)} %bitcast.53), calls=%async_computation.2 | async-start | bytes 393216 | tf_op jit(solution)/shard_map/all_to_all | solution.py:43
  140.1 0.1 copy.11
  140.2 7.2 %all-to-all-done.1 = bf16[4,96,256]{2,1,0:T(8,128)(2,1)S(1)} async-done(((bf16[4,96,256]{2,1,0:T(8,128)(2,1)}), bf16[4,96,256]{2,1,0:T(8,128)(2,1)S(1)}, u32[]{:S(2)}, u32[]{:S(2)}) %all-to-all-start.1) | async-done | bytes 196640 | tf_op jit(solution)/shard_map/all_to_all | solution.py:43
  147.4 2.0 %gather_fusion = f32[256,256]{1,0:T(8,128)S(1)} fusion(f32[4,96,256]{2,1,0:T(8,128)S(1)} %convert_element_type.47, s32[256]{0:T(256)S(1)} %bitcast.50), kind=kCustom, calls=%fused_computation | custom fusion | bytes 526336 | tf_op jit(solution)/shard_map/gather | solution.py:47
  149.4 0.1 reshape.86
  149.6 1.0 multiply_reduce_fusion
  (12 shorter events, 0.2 us)
Async XLA Ops:
  6.5 128.9 %reduce-scatter.2.cloned.1.call-start = ((), (), s32[]{:S(2)}) async-start(), calls=%async_computation.3 | async-start | bytes 1769472 | tf_op jit(solution)/shard_map/reduce_scatter | solution.py:39
  86.2 53.9 %copy-start = (f32[128,2]{0,1:T(2,128)S(1)}, f32[128,2]{0,1:T(2,128)}, u32[]{:S(2)}) copy-start(f32[128,2]{0,1:T(2,128)} %param.10) | copy-start | bytes 3076
  135.4 11.9 %all-to-all-start.1 = ((bf16[4,96,256]{2,1,0:T(8,128)(2,1)}), bf16[4,96,256]{2,1,0:T(8,128)(2,1)S(1)}, u32[]{:S(2)}, u32[]{:S(2)}) async-start(bf16[4,96,256]{2,1,0:T(8,128)(2,1)} %bitcast.53), calls=%async_computation.2 | async-start | bytes 393216 | tf_op jit(solution)/shard_map/all_to_all | solution.py:43
Sparse Core Ops, SparseCore 0:
  98.0 37.4 reduce-scatter.1
where the time goes:
time: 158 us; the launch traced here: 157 us
  waiting for transfers between devices  44.8 us (28%)
  blocking collectives  43.1 us (27%)
  local copies, waits for them, and re-layouts  28.1 us (18%)
  matrix products  18.4 us (12%)
  between operations  13.5 us (9%)
  other arithmetic  4.92 us (3%)
  starting transfers between devices  4.61 us (3%)
    all_to_all x1, blocking collectives, local(): lax.all_to_all(outgoing, 'ep', split_axis=0, concat_axis=0, tiled=True)  43.1 us
    reduce_scatter x1, waiting for transfers between devices, local(): lax.psum_scatter(term.astype(jnp.float32).astype(jnp.bfloat16), 'tp', sca...  37.6 us
    scatter x1, local copies, waits for them, and re-layouts, local(): outgoing = jnp.zeros((ep_count, capacity, width), jnp.bfloat16).at[route_...  23.1 us
    dot_general x1, matrix products, local(): lax.dot_general(down_local, hidden, (((0,), (1,)), ((), ())), preferred_e...  11.6 us
    all_to_all x1, waiting for transfers between devices, local(): lax.all_to_all(back.astype(jnp.bfloat16), 'ep', split_axis=0, concat_axis...  7.19 us
    dot_general x1, matrix products, local(): jnp.dot(merged_rows, gate_proj[0], preferred_element_type=jnp.float32)  6.79 us
    all_to_all x1, starting transfers between devices, local(): lax.all_to_all(back.astype(jnp.bfloat16), 'ep', split_axis=0, concat_axis...  4.61 us
  transfers between devices with their start and end apart: 2, of which 2 were waited for; matrix products, arithmetic and copies ran while one was open for 0% of the time, Pallas kernels for 0%

commit v1 on v0

--- a/solution.py
+++ b/solution.py
@@ -1,7 +1,270 @@
+import functools
+
 import jax
 import jax.numpy as jnp
 from jax import lax
+from jax.experimental import pallas as pl
+from jax.experimental.pallas import tpu as pltpu
 from jax.sharding import PartitionSpec as P
+
+MESH = pl.DeviceIdType.MESH
+F32, BF16 = jnp.float32, jnp.bfloat16
+
+
+def dot(a, b):
+    return jnp.dot(a, b, preferred_element_type=F32)
+
+
+def fused(ep, cap, share, chunk, tok, gain, ids, wts, gate_h, up_h, down_h, out, *scratch):
+    (normed, pick, rows, outbox, gate_w, up_w, down_w, hidden, to_sib, from_sib, acc, sent, from_diag,
+     from_x, from_y, relay, final, back, wsem, ssem, rsem) = scratch
+    toks, width = tok.shape
+    topk = ids.shape[0]
+    hid = hidden.shape[1]
+    total = ep * cap
+    half = total // 2
+    e = lax.axis_index("ep")
+    j = lax.axis_index("tp")
+    c, x, y = j % 2, (j // 2) % 2, j // 4
+
+    def at(yy, xx, cc):
+        return (yy * 2 + xx) * 2 + cc
+
+    spots = [(y, x), (y, 1 - x), (1 - y, x), (1 - y, 1 - x)]
+
+    def cols(m, core):
+        return pl.ds(pl.multiple_of(at(*spots[m], core) * share, share), share)
+
+    x_dev = (e, at(y, 1 - x, c))
+    y_dev = (e, at(1 - y, x, c))
+    sib = (e, at(y, x, 1 - c))
+    dists = list(range(1, ep))
+    near = sorted(dists, key=lambda d: min(d, ep - d))
+
+    loads = [
+        pltpu.make_async_copy(h.at[0], v, wsem.at[i])
+        for i, (h, v) in enumerate(((gate_h, gate_w), (up_h, up_w), (down_h, down_w)))
+    ]
+    for load in loads:
+        load.start()
+    barrier = pltpu.get_barrier_semaphore()
+    greeted = [((e + d) % ep, j) for d in dists] + [x_dev, y_dev, sib]
+    for dev in greeted:
+        pl.semaphore_signal(barrier, inc=1, device_id=dev, device_id_type=MESH)
+
+    count = [0]
+    started = []
+
+    def remote(src, dst, dev):
+        k = count[0]
+        count[0] += 1
+        copy = pltpu.make_async_remote_copy(
+            src_ref=src, dst_ref=dst, send_sem=ssem.at[k], recv_sem=rsem.at[k],
+            device_id=dev, device_id_type=MESH,
+        )
+        started.append(copy)
+        copy.start()
+        return copy
+
+    values = tok[...].astype(F32)
+    mean_square = jnp.mean(values * values, axis=-1, keepdims=True)
+    normed[...] = (values * lax.rsqrt(mean_square + 1e-06) * gain[...]).astype(BF16)
+    experts = lax.broadcasted_iota(jnp.int32, (8 * ((ep + 7) // 8), toks), 0)
+    named = jnp.zeros(experts.shape, jnp.bool_)
+    for k in range(topk):
+        named = named | (ids[k : k + 1, :] == experts)
+    named = jnp.where(named, 1.0, 0.0)
+    before = (
+        lax.broadcasted_iota(jnp.int32, (toks, toks), 0)
+        < lax.broadcasted_iota(jnp.int32, (toks, toks), 1)
+    )
+    slot = dot(named.astype(BF16), jnp.where(before, 1.0, 0.0).astype(BF16))
+    place = jnp.where(named > 0.5, slot, -1.0)
+    slots = lax.broadcasted_iota(jnp.int32, (cap, toks), 0).astype(F32)
+    for s in range(ep):
+        pick[s] = jnp.where(place[s : s + 1, :] == slots, 1.0, 0.0).astype(BF16)
+    mine = cols(0, c)
+    for d in dists:
+        outbox[d - 1] = dot(pick[(e + d) % ep], normed[:, mine]).astype(BF16)
+
+    pl.semaphore_wait(barrier, len(greeted))
+    over_z = {}
+    for d in sorted(dists, key=lambda d: -min(d, ep - d)):
+        over_z[d] = remote(outbox.at[d - 1], rows.at[e, :, mine], ((e + d) % ep, j))
+    rows[e] = dot(pick[e], normed[...]).astype(BF16)
+
+    along_x, along_y, diag_1, diag_2, over_d2d = {}, {}, {}, {}, []
+    quarter = share // 2
+
+    def piece(s, m, part=None):
+        if part is None:
+            return rows.at[s, :, cols(m, c)]
+        start = pl.multiple_of(at(*spots[m], c) * share + part * quarter, quarter)
+        return rows.at[s, :, pl.ds(start, quarter)]
+
+    for t in range(len(near) + 2):
+        if t < len(near):
+            d = near[t]
+            s = (e + ep - d) % ep
+            over_z[d].wait_recv()
+            along_x[d] = remote(piece(s, 0), piece(s, 0), x_dev)
+            along_y[d] = remote(piece(s, 0), piece(s, 0), y_dev)
+            over_d2d.append(remote(piece(s, 0), piece(s, 0), sib))
+        if 0 <= t - 1 < len(near):
+            d = near[t - 1]
+            s = (e + ep - d) % ep
+            along_x[d].wait_recv()
+            diag_1[d] = remote(piece(s, 1, 0), piece(s, 1, 0), y_dev)
+            over_d2d.append(remote(piece(s, 1), piece(s, 1), sib))
+            along_y[d].wait_recv()
+            diag_2[d] = remote(piece(s, 2, 1), piece(s, 2, 1), x_dev)
+            over_d2d.append(remote(piece(s, 2), piece(s, 2), sib))
+        if 0 <= t - 2:
+            d = near[t - 2]
+            s = (e + ep - d) % ep
+            diag_1[d].wait_recv()
+            diag_2[d].wait_recv()
+            over_d2d.append(remote(piece(s, 3), piece(s, 3), sib))
+    loads[0].wait()
+    loads[1].wait()
+    for copy in over_d2d:
+        copy.wait_recv()
+
+    @pl.loop(0, hid // chunk)
+    def _(n):
+        at_n = pl.ds(pl.multiple_of(n * chunk, chunk), chunk)
+        held = rows[...].reshape(total, width)
+        gate_act = dot(held, gate_w[:, at_n])
+        up_act = dot(held, up_w[:, at_n])
+        hidden[:, at_n] = (gate_act / (1.0 + jnp.exp(-gate_act)) * up_act).astype(BF16)
+
+    loads[2].wait()
+    pair = {}
+
+    def compute(m):
+        to_sib[m] = dot(hidden[...], down_w[:, cols(m, 1 - c)]).astype(BF16)
+        pair[m] = remote(to_sib.at[m], from_sib.at[m], sib)
+        acc[m] = dot(hidden[...], down_w[:, cols(m, c)])
+
+    def joined(m):
+        pair[m].wait_recv()
+        return acc[m] + from_sib[m].astype(F32)
+
+    low, high = pl.ds(0, half), pl.ds(half, half)
+    compute(3)
+    compute(1)
+    sent[0] = joined(3).astype(BF16)
+    diag_a = remote(sent.at[0, low], from_diag.at[0], x_dev)
+    diag_b = remote(sent.at[0, high], from_diag.at[1], y_dev)
+    compute(2)
+    along = joined(1)
+    sent[1, :half] = along[:half].astype(BF16)
+    acc[1] = along
+    x_a = remote(sent.at[1, low], from_x.at[0], x_dev)
+    compute(0)
+    along = joined(2)
+    sent[2, half:] = along[half:].astype(BF16)
+    acc[2] = along
+    y_b = remote(sent.at[2, high], from_y.at[1], y_dev)
+    diag_a.wait_recv()
+    relay[0] = (acc[2, :half] + from_diag[0].astype(F32)).astype(BF16)
+    y_a = remote(relay.at[0], from_y.at[0], y_dev)
+    diag_b.wait_recv()
+    relay[1] = (acc[1, half:] + from_diag[1].astype(F32)).astype(BF16)
+    x_b = remote(relay.at[1], from_x.at[1], x_dev)
+    acc[0] = joined(0)
+    for i, (one, two) in enumerate(((x_a, y_a), (y_b, x_b))):
+        one.wait_recv()
+        two.wait_recv()
+        part = acc[0, i * half : (i + 1) * half] + from_x[i].astype(F32) + from_y[i].astype(F32)
+        final[i * ep // 2 : (i + 1) * ep // 2] = part.astype(BF16).reshape(ep // 2, cap, share)
+
+    homeward = {}
+    for d in sorted(dists, key=lambda d: -min(d, ep - d)):
+        s = (e + d) % ep
+        homeward[d] = remote(final.at[s], back.at[e], (s, j))
+    eye = (
+        lax.broadcasted_iota(jnp.int32, (toks, toks), 0)
+        == lax.broadcasted_iota(jnp.int32, (toks, toks), 1)
+    )
+
+    def weighted(expert, value):
+        scale = jnp.zeros((1, toks), F32)
+        for k in range(topk):
+            scale = scale + jnp.where(ids[k : k + 1, :] == expert, wts[k : k + 1, :], 0.0)
+        scale = jnp.sum(jnp.where(eye, scale, 0.0), axis=1, keepdims=True)
+        got = lax.dot_general(
+            pick[expert], value, (((0,), (0,)), ((), ())), preferred_element_type=F32
+        )
+        return scale * got
+
+    mixed = weighted(e, final[e])
+    for d in near:
+        expert = (e + ep - d) % ep
+        homeward[d].wait_recv()
+        mixed = mixed + weighted(expert, back[expert])
+    out[...] = mixed.astype(out.dtype)
+    for copy in started:
+        copy.wait_send()
+
+
+def local_fused(tokens, norm_gain, route_ids, route_weights, gate_proj, up_proj, down_proj):
+    ep = lax.axis_size("ep")
+    tp = lax.axis_size("tp")
+    toks, width = tokens.shape
+    topk = route_ids.shape[1]
+    hid = gate_proj.shape[2]
+    cap = capacity_of(toks, topk, ep)
+    share = width // tp
+    total = ep * cap
+    chunk = next(n for n in (256, 128) if hid % n == 0)
+    others = ep - 1
+    copies = 10 * others + 4 + 6 + others
+    vmem = pl.BlockSpec(memory_space=pltpu.VMEM)
+    hbm = pl.BlockSpec(memory_space=pltpu.HBM)
+    flops = 6 * total * width * hid
+    return pl.pallas_call(
+        functools.partial(fused, ep, cap, share, chunk),
+        out_shape=jax.ShapeDtypeStruct((toks, share), BF16),
+        in_specs=[vmem] * 4 + [hbm] * 3,
+        out_specs=vmem,
+        scratch_shapes=[
+            pltpu.VMEM((toks, width), BF16),
+            pltpu.VMEM((ep, cap, toks), BF16),
+            pltpu.VMEM((ep, cap, width), BF16),
+            pltpu.VMEM((others, cap, share), BF16),
+            pltpu.VMEM((width, hid), BF16),
+            pltpu.VMEM((width, hid), BF16),
+            pltpu.VMEM((hid, width), BF16),
+            pltpu.VMEM((total, hid), BF16),
+            pltpu.VMEM((4, total, share), BF16),
+            pltpu.VMEM((4, total, share), BF16),
+            pltpu.VMEM((4, total, share), F32),
+            pltpu.VMEM((3, total, share), BF16),
+            pltpu.VMEM((2, total // 2, share), BF16),
+            pltpu.VMEM((2, total // 2, share), BF16),
+            pltpu.VMEM((2, total // 2, share), BF16),
+            pltpu.VMEM((2, total // 2, share), BF16),
+            pltpu.VMEM((ep, cap, share), BF16),
+            pltpu.VMEM((ep, cap, share), BF16),
+            pltpu.SemaphoreType.DMA((3,)),
+            pltpu.SemaphoreType.DMA((copies,)),
+            pltpu.SemaphoreType.DMA((copies,)),
+        ],
+        compiler_params=pltpu.CompilerParams(
+            collective_id=0, has_side_effects=True, vmem_limit_bytes=56 * 1024 * 1024
+        ),
+        cost_estimate=pl.CostEstimate(
+            flops=flops, bytes_accessed=6 * width * hid, transcendentals=total * hid
+        ),
+    )(
+        tokens, norm_gain.reshape(1, width), route_ids.T, route_weights.T,
+        gate_proj, up_proj, down_proj,
+    )
+
+
+def capacity_of(tok_rows, topk, ep_count):
+    return min(tok_rows, (3 * tok_rows * topk + 2 * ep_count - 1) // (2 * ep_count))
 
 
 def local(tokens, norm_gain, route_ids, route_weights, gate_proj, up_proj, down_proj):
@@ -59,6 +322,17 @@
         P("ep", None, "tp"),
         P("ep", "tp", None),
     )
-    return jax.shard_map(
-        local, mesh=mesh, in_specs=placed, out_specs=P("ep", "tp"), check_vma=False
-    )
+    ep, tp = mesh.shape["ep"], mesh.shape["tp"]
+
+    def whole(tokens, norm_gain, route_ids, route_weights, gate_proj, up_proj, down_proj):
+        toks, width = tokens.shape[0] // ep, tokens.shape[1]
+        cap = capacity_of(toks, route_ids.shape[1], ep)
+        hid = gate_proj.shape[2] // tp
+        cube = tp == 2**3 and ep % 2 == 0
+        fits = width % (tp * 256) == 0 and hid % 128 == 0 and cap % 16 == 0 and toks % 128 == 0
+        body = local_fused if cube and fits else local
+        return jax.shard_map(
+            body, mesh=mesh, in_specs=placed, out_specs=P("ep", "tp"), check_vma=False
+        )(tokens, norm_gain, route_ids, route_weights, gate_proj, up_proj, down_proj)
+
+    return whole

time: 158 us -> 48.4 us (0.31)
  Pallas kernels: 0 us -> 46.8 us
  waiting for transfers between devices: 44.8 us -> 0 us
  blocking collectives: 43.1 us -> 0 us
  local copies, waits for them, and re-layouts: 28.1 us -> 1.47 us
  matrix products: 18.4 us -> 0 us
  between operations: 13.5 us -> 0.01 us
  other arithmetic: 4.92 us -> 0 us
  starting transfers between devices: 4.61 us -> 0 us
    pallas_call x0 -> x1, Pallas kernels: none -> 46.8 us  [local_fused(): pl.pallas_call(functools.partial(fused, ep, cap, share, chunk), out_shape...]
    all_to_all x1 -> x0, blocking collectives: 43.1 us -> none  [local(): lax.all_to_all(outgoing, 'ep', split_axis=0, concat_axis=0, tiled=True)]
    reduce_scatter x1 -> x0, waiting for transfers between devices: 37.6 us -> none  [local(): lax.psum_scatter(term.astype(jnp.float32).astype(jnp.bfloat16), 'tp', sca...]
    scatter x1 -> x0, local copies, waits for them, and re-layouts: 23.1 us -> none  [local(): outgoing = jnp.zeros((ep_count, capacity, width), jnp.bfloat16).at[route_...]
    dot_general x2 -> x0, matrix products: 18.4 us -> none  [the longest x1 11.6 us: local(): lax.dot_general(down_local, hidden, (((0,), (1,)), ((), ())), preferred_e...]
    all_to_all x1 -> x0, waiting for transfers between devices: 7.19 us -> none  [local(): lax.all_to_all(back.astype(jnp.bfloat16), 'ep', split_axis=0, concat_axis...]
    all_to_all x1 -> x0, starting transfers between devices: 4.61 us -> none  [local(): lax.all_to_all(back.astype(jnp.bfloat16), 'ep', split_axis=0, concat_axis...]
    reduce_sum x3 -> x0, other arithmetic: 2.29 us -> none  [the longest x1 1.23 us: local(): mean_square = jnp.mean(values * values, axis=-1, keepdims=True)]
  transfers between devices with their start and end apart: 2 -> 0, of which waited for: 2 -> 0; matrix products, arithmetic and copies ran while one was open for 0% -> 0% of each run, Pallas kernels for 0% -> 0%
where the time goes in v1:
time: 48.4 us; the launch traced here: 48.3 us
  Pallas kernels  46.8 us (97%)
  local copies, waits for them, and re-layouts  1.47 us (3%)
    pallas_call x1, Pallas kernels, local_fused(): pl.pallas_call(functools.partial(fused, ep, cap, share, chunk), out_shape...  46.8 us
    unnamed x1, local copies, waits for them, and re-layouts  1.47 us

profile of v1, /device:TPU:0, one launch (start us, length us, event | category | flops | bytes accessed | tf_op | source)
XLA Modules:
  0.0 48.3 jit_solution(10309966643007219907)
XLA Ops:
  0.0 46.8 %shard_map.73 = bf16[128,256]{1,0:T(8,128)(2,1)} custom-call(bf16[128,2048]{1,0:T(8,128)(2,1)} %tok.1, f32[1,2048]{1,0:T(1,128)} %bitcast.3, s32[2,128]{1,0:T(2,128)} %bitcast.4, f32[2,128]{1,0:T(2,128)} %bitcast.5, bf16[1,2048,1536]{2,1,0:T(8,128)(2,1)} %gate_h.1, bf16[1,2048,1536]{2,1,0:T(8,128)(2,1)} %up_h.1, bf16[1,1536,2048]{2,1,0:T(8,128)(2,1)} %down_h.1), custom_call_target="tpu_custom_call" | custom-call | flops 7247757312 | bytes 18874368 | tf_op jit(solution)/shard_map/pallas_call | solution.py:226
  46.8 1.5 %copy.9 = bf16[128,256]{1,0:T(8,128)(2,1)} copy(bf16[128,256]{1,0:T(8,128)(2,1)} %shard_map.73) | data formatting | bytes 131072

commit v2 on v1

--- a/solution.py
+++ b/solution.py
@@ -20,9 +20,7 @@
      from_x, from_y, relay, final, back, wsem, ssem, rsem) = scratch
     toks, width = tok.shape
     topk = ids.shape[0]
-    hid = hidden.shape[1]
-    total = ep * cap
-    half = total // 2
+    hid = hidden.shape[2]
     e = lax.axis_index("ep")
     j = lax.axis_index("tp")
     c, x, y = j % 2, (j // 2) % 2, j // 4
@@ -38,8 +36,6 @@
     x_dev = (e, at(y, 1 - x, c))
     y_dev = (e, at(1 - y, x, c))
     sib = (e, at(y, x, 1 - c))
-    dists = list(range(1, ep))
-    near = sorted(dists, key=lambda d: min(d, ep - d))
 
     loads = [
         pltpu.make_async_copy(h.at[0], v, wsem.at[i])
@@ -48,7 +44,7 @@
     for load in loads:
         load.start()
     barrier = pltpu.get_barrier_semaphore()
-    greeted = [((e + d) % ep, j) for d in dists] + [x_dev, y_dev, sib]
+    greeted = [((e + d) % ep, j) for d in range(1, ep)] + [x_dev, y_dev, sib]
     for dev in greeted:
         pl.semaphore_signal(barrier, inc=1, device_id=dev, device_id_type=MESH)
 
@@ -66,10 +62,16 @@
         copy.start()
         return copy
 
+    near = e + 1 - 2 * (e % 2)
+    peers = [e, near, (e + 2) % ep, (near + 2) % ep]
+
     values = tok[...].astype(F32)
     mean_square = jnp.mean(values * values, axis=-1, keepdims=True)
     normed[...] = (values * lax.rsqrt(mean_square + 1e-06) * gain[...]).astype(BF16)
-    experts = lax.broadcasted_iota(jnp.int32, (8 * ((ep + 7) // 8), toks), 0)
+    turn = lax.broadcasted_iota(jnp.int32, (8, toks), 0)
+    experts = jnp.full((8, toks), -1, jnp.int32)
+    for i in range(ep):
+        experts = jnp.where(turn == i, peers[i], experts)
     named = jnp.zeros(experts.shape, jnp.bool_)
     for k in range(topk):
         named = named | (ids[k : k + 1, :] == experts)
@@ -81,128 +83,161 @@
     slot = dot(named.astype(BF16), jnp.where(before, 1.0, 0.0).astype(BF16))
     place = jnp.where(named > 0.5, slot, -1.0)
     slots = lax.broadcasted_iota(jnp.int32, (cap, toks), 0).astype(F32)
-    for s in range(ep):
-        pick[s] = jnp.where(place[s : s + 1, :] == slots, 1.0, 0.0).astype(BF16)
+    for i in range(ep):
+        pick[i] = jnp.where(place[i : i + 1, :] == slots, 1.0, 0.0).astype(BF16)
     mine = cols(0, c)
-    for d in dists:
-        outbox[d - 1] = dot(pick[(e + d) % ep], normed[:, mine]).astype(BF16)
+    for i in range(1, ep):
+        outbox[i - 1] = dot(pick[i], normed[:, mine]).astype(BF16)
 
     pl.semaphore_wait(barrier, len(greeted))
     over_z = {}
-    for d in sorted(dists, key=lambda d: -min(d, ep - d)):
-        over_z[d] = remote(outbox.at[d - 1], rows.at[e, :, mine], ((e + d) % ep, j))
-    rows[e] = dot(pick[e], normed[...]).astype(BF16)
-
-    along_x, along_y, diag_1, diag_2, over_d2d = {}, {}, {}, {}, []
+    for i in range(1, ep):
+        over_z[i] = remote(outbox.at[i - 1], rows.at[i, :, mine], (peers[i], j))
+    rows[0] = dot(pick[0], normed[...]).astype(BF16)
+
+    along_x, along_y, diag_1, diag_2 = {}, {}, {}, {}
+    over_d2d = {i: [] for i in range(1, ep)}
     quarter = share // 2
 
-    def piece(s, m, part=None):
+    def piece(i, m, part=None):
         if part is None:
-            return rows.at[s, :, cols(m, c)]
+            return rows.at[i, :, cols(m, c)]
         start = pl.multiple_of(at(*spots[m], c) * share + part * quarter, quarter)
-        return rows.at[s, :, pl.ds(start, quarter)]
-
-    for t in range(len(near) + 2):
-        if t < len(near):
-            d = near[t]
-            s = (e + ep - d) % ep
-            over_z[d].wait_recv()
-            along_x[d] = remote(piece(s, 0), piece(s, 0), x_dev)
-            along_y[d] = remote(piece(s, 0), piece(s, 0), y_dev)
-            over_d2d.append(remote(piece(s, 0), piece(s, 0), sib))
-        if 0 <= t - 1 < len(near):
-            d = near[t - 1]
-            s = (e + ep - d) % ep
-            along_x[d].wait_recv()
-            diag_1[d] = remote(piece(s, 1, 0), piece(s, 1, 0), y_dev)
-            over_d2d.append(remote(piece(s, 1), piece(s, 1), sib))
-            along_y[d].wait_recv()
-            diag_2[d] = remote(piece(s, 2, 1), piece(s, 2, 1), x_dev)
-            over_d2d.append(remote(piece(s, 2), piece(s, 2), sib))
-        if 0 <= t - 2:
-            d = near[t - 2]
-            s = (e + ep - d) % ep
-            diag_1[d].wait_recv()
-            diag_2[d].wait_recv()
-            over_d2d.append(remote(piece(s, 3), piece(s, 3), sib))
+        return rows.at[i, :, pl.ds(start, quarter)]
+
+    def spread(i):
+        over_z[i].wait_recv()
+        along_x[i] = remote(piece(i, 0), piece(i, 0), x_dev)
+        along_y[i] = remote(piece(i, 0), piece(i, 0), y_dev)
+        over_d2d[i].append(remote(piece(i, 0), piece(i, 0), sib))
+
+    def forward(i):
+        along_x[i].wait_recv()
+        diag_1[i] = remote(piece(i, 1, 0), piece(i, 1, 0), y_dev)
+        along_y[i].wait_recv()
+        diag_2[i] = remote(piece(i, 2, 1), piece(i, 2, 1), x_dev)
+        over_d2d[i].append(remote(piece(i, 1), piece(i, 1), sib))
+        over_d2d[i].append(remote(piece(i, 2), piece(i, 2), sib))
+
+    def across(i):
+        diag_1[i].wait_recv()
+        diag_2[i].wait_recv()
+        over_d2d[i].append(remote(piece(i, 3), piece(i, 3), sib))
+
+    def gathered(i):
+        for copy in over_d2d[i]:
+            copy.wait_recv()
+
+    pace = hid // chunk
+
+    def gate_up(g, n):
+        at_n = pl.ds(n * chunk, chunk)
+        held = rows[2 * g : 2 * g + 2].reshape(2 * cap, width)
+        gate_act = dot(held, gate_w[:, at_n])
+        up_act = dot(held, up_w[:, at_n])
+        hidden[g, :, at_n] = (gate_act / (1.0 + jnp.exp(-gate_act)) * up_act).astype(BF16)
+
+    def gate_up_with(g, steps):
+        for n in range(pace):
+            gate_up(g, n)
+            first = n * len(steps) // pace
+            for step in steps[first : (n + 1) * len(steps) // pace]:
+                step()
+
+    pair, sends = {}, {}
+    low, high = pl.ds(0, cap), pl.ds(cap, cap)
+
+    def compute(g, m):
+        to_sib[g, m] = dot(hidden[g], down_w[:, cols(m, 1 - c)]).astype(BF16)
+        pair[g, m] = remote(to_sib.at[g, m], from_sib.at[g, m], sib)
+        acc[g, m] = dot(hidden[g], down_w[:, cols(m, c)])
+
+    def join(g, m):
+        pair[g, m].wait_recv()
+        along = acc[g, m] + from_sib[g, m].astype(F32)
+        if m == 3:
+            sent[g, 0] = along.astype(BF16)
+            sends[g, "diag_a"] = remote(sent.at[g, 0, low], from_diag.at[g, 0], x_dev)
+            sends[g, "diag_b"] = remote(sent.at[g, 0, high], from_diag.at[g, 1], y_dev)
+            return
+        acc[g, m] = along
+        if m == 1:
+            sent[g, 1, :cap] = along[:cap].astype(BF16)
+            sends[g, "x_a"] = remote(sent.at[g, 1, low], from_x.at[g, 0], x_dev)
+        if m == 2:
+            sent[g, 2, cap:] = along[cap:].astype(BF16)
+            sends[g, "y_b"] = remote(sent.at[g, 2, high], from_y.at[g, 1], y_dev)
+
+    def pass_on(g):
+        sends[g, "diag_a"].wait_recv()
+        relay[g, 0] = (acc[g, 2, :cap] + from_diag[g, 0].astype(F32)).astype(BF16)
+        sends[g, "y_a"] = remote(relay.at[g, 0], from_y.at[g, 0], y_dev)
+        sends[g, "diag_b"].wait_recv()
+        relay[g, 1] = (acc[g, 1, cap:] + from_diag[g, 1].astype(F32)).astype(BF16)
+        sends[g, "x_b"] = remote(relay.at[g, 1], from_x.at[g, 1], x_dev)
+
+    def down(g):
+        compute(g, 3)
+        compute(g, 1)
+        join(g, 3)
+        compute(g, 2)
+        join(g, 1)
+        compute(g, 0)
+        join(g, 2)
+
+    homeward = {}
+
+    def finish(g):
+        for i, (one, two) in enumerate((("x_a", "y_a"), ("y_b", "x_b"))):
+            sends[g, one].wait_recv()
+            sends[g, two].wait_recv()
+            part = acc[g, 0, i * cap : (i + 1) * cap]
+            part = part + from_x[g, i].astype(F32) + from_y[g, i].astype(F32)
+            p = 2 * g + i
+            final[p] = part.astype(BF16)
+            if p:
+                homeward[p] = remote(final.at[p], back.at[p], (peers[p], j))
+
+    spread(1)
+    forward(1)
+    spread(2)
+    across(1)
+    spread(3)
     loads[0].wait()
     loads[1].wait()
-    for copy in over_d2d:
-        copy.wait_recv()
-
-    @pl.loop(0, hid // chunk)
-    def _(n):
-        at_n = pl.ds(pl.multiple_of(n * chunk, chunk), chunk)
-        held = rows[...].reshape(total, width)
-        gate_act = dot(held, gate_w[:, at_n])
-        up_act = dot(held, up_w[:, at_n])
-        hidden[:, at_n] = (gate_act / (1.0 + jnp.exp(-gate_act)) * up_act).astype(BF16)
-
+    gathered(1)
+    gate_up_with(0, [
+        lambda: forward(2), lambda: forward(3), lambda: across(2), lambda: across(3),
+    ])
     loads[2].wait()
-    pair = {}
-
-    def compute(m):
-        to_sib[m] = dot(hidden[...], down_w[:, cols(m, 1 - c)]).astype(BF16)
-        pair[m] = remote(to_sib.at[m], from_sib.at[m], sib)
-        acc[m] = dot(hidden[...], down_w[:, cols(m, c)])
-
-    def joined(m):
-        pair[m].wait_recv()
-        return acc[m] + from_sib[m].astype(F32)
-
-    low, high = pl.ds(0, half), pl.ds(half, half)
-    compute(3)
-    compute(1)
-    sent[0] = joined(3).astype(BF16)
-    diag_a = remote(sent.at[0, low], from_diag.at[0], x_dev)
-    diag_b = remote(sent.at[0, high], from_diag.at[1], y_dev)
-    compute(2)
-    along = joined(1)
-    sent[1, :half] = along[:half].astype(BF16)
-    acc[1] = along
-    x_a = remote(sent.at[1, low], from_x.at[0], x_dev)
-    compute(0)
-    along = joined(2)
-    sent[2, half:] = along[half:].astype(BF16)
-    acc[2] = along
-    y_b = remote(sent.at[2, high], from_y.at[1], y_dev)
-    diag_a.wait_recv()
-    relay[0] = (acc[2, :half] + from_diag[0].astype(F32)).astype(BF16)
-    y_a = remote(relay.at[0], from_y.at[0], y_dev)
-    diag_b.wait_recv()
-    relay[1] = (acc[1, half:] + from_diag[1].astype(F32)).astype(BF16)
-    x_b = remote(relay.at[1], from_x.at[1], x_dev)
-    acc[0] = joined(0)
-    for i, (one, two) in enumerate(((x_a, y_a), (y_b, x_b))):
-        one.wait_recv()
-        two.wait_recv()
-        part = acc[0, i * half : (i + 1) * half] + from_x[i].astype(F32) + from_y[i].astype(F32)
-        final[i * ep // 2 : (i + 1) * ep // 2] = part.astype(BF16).reshape(ep // 2, cap, share)
-
-    homeward = {}
-    for d in sorted(dists, key=lambda d: -min(d, ep - d)):
-        s = (e + d) % ep
-        homeward[d] = remote(final.at[s], back.at[e], (s, j))
+    down(0)
+    gathered(2)
+    gathered(3)
+    gate_up_with(1, [lambda: pass_on(0), lambda: join(0, 0), lambda: finish(0)])
+    down(1)
+    pass_on(1)
+    join(1, 0)
+    finish(1)
+
     eye = (
         lax.broadcasted_iota(jnp.int32, (toks, toks), 0)
         == lax.broadcasted_iota(jnp.int32, (toks, toks), 1)
     )
 
-    def weighted(expert, value):
+    def weighted(i, value):
         scale = jnp.zeros((1, toks), F32)
         for k in range(topk):
-            scale = scale + jnp.where(ids[k : k + 1, :] == expert, wts[k : k + 1, :], 0.0)
+            scale = scale + jnp.where(ids[k : k + 1, :] == peers[i], wts[k : k + 1, :], 0.0)
         scale = jnp.sum(jnp.where(eye, scale, 0.0), axis=1, keepdims=True)
         got = lax.dot_general(
-            pick[expert], value, (((0,), (0,)), ((), ())), preferred_element_type=F32
+            pick[i], value, (((0,), (0,)), ((), ())), preferred_element_type=F32
         )
         return scale * got
 
-    mixed = weighted(e, final[e])
-    for d in near:
-        expert = (e + ep - d) % ep
-        homeward[d].wait_recv()
-        mixed = mixed + weighted(expert, back[expert])
+    mixed = weighted(0, final[0])
+    for i in range(1, ep):
+        homeward[i].wait_recv()
+        mixed = mixed + weighted(i, back[i])
     out[...] = mixed.astype(out.dtype)
     for copy in started:
         copy.wait_send()
@@ -219,7 +254,7 @@
     total = ep * cap
     chunk = next(n for n in (256, 128) if hid % n == 0)
     others = ep - 1
-    copies = 10 * others + 4 + 6 + others
+    copies = 9 * others + 2 * (4 + 6) + others
     vmem = pl.BlockSpec(memory_space=pltpu.VMEM)
     hbm = pl.BlockSpec(memory_space=pltpu.HBM)
     flops = 6 * total * width * hid
@@ -236,15 +271,15 @@
             pltpu.VMEM((width, hid), BF16),
             pltpu.VMEM((width, hid), BF16),
             pltpu.VMEM((hid, width), BF16),
-            pltpu.VMEM((total, hid), BF16),
-            pltpu.VMEM((4, total, share), BF16),
-            pltpu.VMEM((4, total, share), BF16),
-            pltpu.VMEM((4, total, share), F32),
-            pltpu.VMEM((3, total, share), BF16),
-            pltpu.VMEM((2, total // 2, share), BF16),
-            pltpu.VMEM((2, total // 2, share), BF16),
-            pltpu.VMEM((2, total // 2, share), BF16),
-            pltpu.VMEM((2, total // 2, share), BF16),
+            pltpu.VMEM((2, 2 * cap, hid), BF16),
+            pltpu.VMEM((2, 4, 2 * cap, share), BF16),
+            pltpu.VMEM((2, 4, 2 * cap, share), BF16),
+            pltpu.VMEM((2, 4, 2 * cap, share), F32),
+            pltpu.VMEM((2, 3, 2 * cap, share), BF16),
+            pltpu.VMEM((2, 2, cap, share), BF16),
+            pltpu.VMEM((2, 2, cap, share), BF16),
+            pltpu.VMEM((2, 2, cap, share), BF16),
+            pltpu.VMEM((2, 2, cap, share), BF16),
             pltpu.VMEM((ep, cap, share), BF16),
             pltpu.VMEM((ep, cap, share), BF16),
             pltpu.SemaphoreType.DMA((3,)),
@@ -328,7 +363,7 @@
         toks, width = tokens.shape[0] // ep, tokens.shape[1]
         cap = capacity_of(toks, route_ids.shape[1], ep)
         hid = gate_proj.shape[2] // tp
-        cube = tp == 2**3 and ep % 2 == 0
+        cube = tp == 2**3 and ep == 2**2
         fits = width % (tp * 256) == 0 and hid % 128 == 0 and cap % 16 == 0 and toks % 128 == 0
         body = local_fused if cube and fits else local
         return jax.shard_map(

time: 48.4 us -> 46.4 us (0.959)
  Pallas kernels: 46.8 us -> 44.8 us
    pallas_call x1, Pallas kernels: 46.8 us -> 44.8 us  [local_fused(): pl.pallas_call(functools.partial(fused, ep, cap, share, chunk), out_shape...]
where the time goes in v2:
time: 46.4 us; the launch traced here: 46.3 us
  Pallas kernels  44.8 us (97%)
  local copies, waits for them, and re-layouts  1.47 us (3%)
    pallas_call x1, Pallas kernels, local_fused(): pl.pallas_call(functools.partial(fused, ep, cap, share, chunk), out_shape...  44.8 us
    unnamed x1, local copies, waits for them, and re-layouts  1.47 us

profile of v2, /device:TPU:0, one launch (start us, length us, event | category | flops | bytes accessed | tf_op | source)
XLA Modules:
  0.0 46.3 jit_solution(14484224555056261549)
XLA Ops:
  0.0 44.8 %shard_map.73 = bf16[128,256]{1,0:T(8,128)(2,1)} custom-call(bf16[128,2048]{1,0:T(8,128)(2,1)} %tok.1, f32[1,2048]{1,0:T(1,128)} %bitcast.3, s32[2,128]{1,0:T(2,128)} %bitcast.4, f32[2,128]{1,0:T(2,128)} %bitcast.5, bf16[1,2048,1536]{2,1,0:T(8,128)(2,1)} %gate_h.1, bf16[1,2048,1536]{2,1,0:T(8,128)(2,1)} %up_h.1, bf16[1,1536,2048]{2,1,0:T(8,128)(2,1)} %down_h.1), custom_call_target="tpu_custom_call" | custom-call | flops 7247757312 | bytes 18874368 | tf_op jit(solution)/shard_map/pallas_call | solution.py:261
  44.8 1.5 %copy.9 = bf16[128,256]{1,0:T(8,128)(2,1)} copy(bf16[128,256]{1,0:T(8,128)(2,1)} %shard_map.73) | data formatting | bytes 131072

commit v3 on v2

--- a/solution.py
+++ b/solution.py
@@ -202,12 +202,11 @@
     forward(1)
     spread(2)
     across(1)
-    spread(3)
     loads[0].wait()
     loads[1].wait()
     gathered(1)
     gate_up_with(0, [
-        lambda: forward(2), lambda: forward(3), lambda: across(2), lambda: across(3),
+        lambda: spread(3), lambda: forward(2), lambda: forward(3), lambda: across(2), lambda: across(3),
     ])
     loads[2].wait()
     down(0)

time: 46.4 us -> 47.7 us (1.028)
  Pallas kernels: 44.8 us -> 46 us
    pallas_call x1, Pallas kernels: 44.8 us -> 46 us  [local_fused(): pl.pallas_call(functools.partial(fused, ep, cap, share, chunk), out_shape...]
where the time goes in v3:
time: 47.7 us; the launch traced here: 47.5 us
  Pallas kernels  46 us (96%)
  local copies, waits for them, and re-layouts  1.47 us (3%)
    pallas_call x1, Pallas kernels, local_fused(): pl.pallas_call(functools.partial(fused, ep, cap, share, chunk), out_shape...  46 us
    unnamed x1, local copies, waits for them, and re-layouts  1.47 us

profile of v3, /device:TPU:0, one launch (start us, length us, event | category | flops | bytes accessed | tf_op | source)
XLA Modules:
  0.0 47.5 jit_solution(13535424202914606663)
XLA Ops:
  0.0 46.0 %shard_map.73 = bf16[128,256]{1,0:T(8,128)(2,1)} custom-call(bf16[128,2048]{1,0:T(8,128)(2,1)} %tok.1, f32[1,2048]{1,0:T(1,128)} %bitcast.3, s32[2,128]{1,0:T(2,128)} %bitcast.4, f32[2,128]{1,0:T(2,128)} %bitcast.5, bf16[1,2048,1536]{2,1,0:T(8,128)(2,1)} %gate_h.1, bf16[1,2048,1536]{2,1,0:T(8,128)(2,1)} %up_h.1, bf16[1,1536,2048]{2,1,0:T(8,128)(2,1)} %down_h.1), custom_call_target="tpu_custom_call" | custom-call | flops 7247757312 | bytes 18874368 | tf_op jit(solution)/shard_map/pallas_call | solution.py:260
  46.0 1.5 %copy.9 = bf16[128,256]{1,0:T(8,128)(2,1)} copy(bf16[128,256]{1,0:T(8,128)(2,1)} %shard_map.73) | data formatting | bytes 131072
